TPU v7x, 32 devices: a whole 2x2x4 slice. The times are simulated.
32 devices in a mesh: kv: 8 (over z, x), tp: 4 (over y, core).
Axes of the slice: x: 2, y: 2, z: 4, core: 2. Of those that a mesh axis runs over, the one named last changes fastest.
Arguments:
- tokens: bfloat16 [384, 2048], P(None, 'kv'), may hold values from -40 to 40
- norm_gain: float32 [2048], P('kv'), may hold values from 0.1 to 1.9
- w_query: bfloat16 [2048, 1024], P('kv', 'tp'), may hold values from -0.088388348 to 0.088388348
- w_key: bfloat16 [2048, 1024], P('kv', 'tp'), may hold values from -0.125 to 0.125
- w_value: bfloat16 [2048, 1024], P('kv', 'tp'), may hold values from -0.125 to 0.125
- w_gate: bfloat16 [2048, 16], replicated, may hold values from -0.125 to 0.125
- gate_bias: float32 [16], replicated, may hold values from -1 to 3
- w_out: bfloat16 [1024, 2048], P('tp', 'kv'), may hold values from -0.1875 to 0.1875
- keys_cache: bfloat16 [24, 4096, 1024], P(None, 'kv', 'tp'), may hold values from -512 to 512
- values_cache: bfloat16 [24, 4096, 1024], P(None, 'kv', 'tp'), may hold values from -6 to 6
- cum_gates: float32 [24, 16, 4096], P(None, 'tp', 'kv'), may hold values from -4496 to 0, as said below
- prior_len: int32 [24], replicated, may hold values from 2048 to 4074, as said below
- accepted: int32 [24], replicated, may hold values from 0 to 6
- parents: int32 [24, 16], replicated, may hold values from -1 to 14, as said below
Outputs:
- mixed_rows: bfloat16 [384, 2048], P('tp', 'kv')
- keys_out: bfloat16 [24, 4096, 1024], P(None, 'kv', 'tp')
- values_out: bfloat16 [24, 4096, 1024], P(None, 'kv', 'tp')
Inputs may be any that keep to these rules, and one draw needn't show every extreme that they name: parents[b, 0] = -1 and 0 <= parents[b, j] < j for later j. prior_len is at least half of 4096, and prior_len + accepted + 16 <= 4096. `cum_gates`: non-increasing along positions.
All inputs are finite; a program needn't handle non-finite values.
Results may differ from a plain program's by a relative error of at most 0.04.
Values may be sent and summed in bfloat16 or wider, within the bound.
A program may use at most 64 MiB of HBM per device.

v0:
```python
import jax
import jax.numpy as jnp
from jax import lax
from jax.sharding import PartitionSpec as P

D = 2048
HEAD = 64
PROPS = 16
masked_score = -1e30
norm_eps = 1e-06


def ancestry(parents):
    columns = jnp.arange(PROPS, dtype=jnp.int32)
    parent_link = (parents[:, :, None] == columns[None, None, :]).astype(jnp.float32)
    reached = jnp.eye(PROPS, dtype=jnp.float32)[None] + parent_link
    for squaring in range(PROPS.bit_length()):
        reached = jnp.minimum(
            jnp.einsum("bij,bjk->bik", reached, reached, precision=lax.Precision.HIGHEST), 1.0
        )
    return reached


def shards(
    tokens,
    norm_gain,
    w_query,
    w_key,
    w_value,
    w_gate,
    gate_bias,
    w_out,
    keys_cache,
    values_cache,
    cum_gates,
    prior_len,
    accepted,
    parents,
):
    row_count = tokens.shape[0]
    column_count = tokens.shape[1]
    seq_count = keys_cache.shape[0]
    length = keys_cache.shape[1]
    head_width = w_query.shape[1]
    head_count = head_width // HEAD
    kv_index = lax.axis_index("kv")
    tp_index = lax.axis_index("tp")
    floats = tokens.astype(jnp.float32)
    square_part = jnp.sum(floats * floats, axis=1)
    scaled = (floats * norm_gain).astype(jnp.bfloat16)
    gate_rows = lax.dynamic_slice_in_dim(w_gate, kv_index * column_count, column_count, 0)
    gate_cols = lax.dynamic_slice_in_dim(gate_rows, tp_index * head_count, head_count, 1)
    gate_part = jnp.dot(scaled, gate_cols, preferred_element_type=jnp.float32)
    bias_local = lax.dynamic_slice_in_dim(gate_bias, tp_index * head_count, head_count, 0)
    query_sum, key_sum, value_sum, gate_sum, square_sum = (
        lax.psum(
            jnp.dot(scaled, w_query, preferred_element_type=jnp.float32).astype(jnp.bfloat16), "kv"
        ).astype(jnp.float32),
        lax.psum(
            jnp.dot(scaled, w_key, preferred_element_type=jnp.float32).astype(jnp.bfloat16), "kv"
        ).astype(jnp.float32),
        lax.psum(
            jnp.dot(scaled, w_value, preferred_element_type=jnp.float32).astype(jnp.bfloat16), "kv"
        ).astype(jnp.float32),
        lax.psum(gate_part.astype(jnp.bfloat16), "kv").astype(jnp.float32),
        lax.psum(square_part.astype(jnp.bfloat16), "kv").astype(jnp.float32),
    )
    inv_rms = lax.rsqrt(square_sum / D + norm_eps)
    queries = (inv_rms[:, None] * query_sum).astype(jnp.bfloat16)
    new_keys = (inv_rms[:, None] * key_sum).astype(jnp.bfloat16)
    new_values = (inv_rms[:, None] * value_sum).astype(jnp.bfloat16)
    log_gates = jax.nn.log_sigmoid(inv_rms[:, None] * gate_sum + bias_local).reshape(
        seq_count, PROPS, head_count
    )
    reached = ancestry(parents)
    tree_gates = jnp.einsum("bij,bjh->bih", reached, log_gates, precision=lax.Precision.HIGHEST)
    filled = prior_len + accepted
    offset = kv_index * length
    local_last = filled - 1 - offset
    owner_mask = (local_last >= 0) & (local_last < length)
    index_last = jnp.broadcast_to(
        jnp.clip(local_last, 0, length - 1)[:, None, None], (seq_count, head_count, 1)
    )
    last_gate = jnp.take_along_axis(cum_gates, index_last, axis=2)[:, :, 0]
    prop_cum = last_gate[:, None, :] + tree_gates
    scale = HEAD ** (-0.5)
    query_four = queries.reshape(seq_count, PROPS, head_count, HEAD)
    keys_four = keys_cache.reshape(seq_count, length, head_count, HEAD)
    values_four = values_cache.reshape(seq_count, length, head_count, HEAD)
    newk_four = new_keys.reshape(seq_count, PROPS, head_count, HEAD)
    newv_four = new_values.reshape(seq_count, PROPS, head_count, HEAD)
    positions = offset + jnp.arange(length, dtype=jnp.int32)
    valid_keys = positions[None, :] < filled[:, None]
    scores = (
        jnp.einsum("bihd,bphd->bhip", query_four, keys_four, preferred_element_type=jnp.float32)
        * scale
    )
    scores = jnp.where(
        valid_keys[:, None, None, :], scores - cum_gates[:, :, None, :], masked_score
    )
    tree_scores = (
        jnp.einsum("bihd,bjhd->bhij", query_four, newk_four, preferred_element_type=jnp.float32)
        * scale
    )
    tree_scores = tree_scores - jnp.transpose(prop_cum, (0, 2, 1))[:, :, None, :]
    tree_live = (reached > 0.5)[:, None, :, :] & owner_mask[:, None, None, None]
    tree_scores = jnp.where(tree_live, tree_scores, masked_score)
    local_max = jnp.maximum(jnp.max(scores, axis=3), jnp.max(tree_scores, axis=3))
    weights = jnp.where(valid_keys[:, None, None, :], jnp.exp(scores - local_max[..., None]), 0.0)
    tree_weights = jnp.where(tree_live, jnp.exp(tree_scores - local_max[..., None]), 0.0)
    local_sum = jnp.sum(weights, axis=3) + jnp.sum(tree_weights, axis=3)
    local_values = jnp.einsum(
        "bhip,bphd->bhid",
        weights.astype(jnp.bfloat16),
        values_four,
        preferred_element_type=jnp.float32,
    )
    local_values = local_values + jnp.einsum(
        "bhij,bjhd->bhid",
        tree_weights.astype(jnp.bfloat16),
        newv_four,
        preferred_element_type=jnp.float32,
    )
    local_values = lax.optimization_barrier(local_values.astype(jnp.bfloat16)).astype(jnp.float32)
    top_score = lax.pmax(local_max, "kv")
    rescale = jnp.exp(local_max - top_score)
    grand_total, weighted = (
        lax.psum((rescale * local_sum).astype(jnp.bfloat16), "kv").astype(jnp.float32),
        lax.psum((rescale[..., None] * local_values).astype(jnp.bfloat16), "kv").astype(
            jnp.float32
        ),
    )
    result = weighted / grand_total[..., None]
    attended = (
        jnp.transpose(result, (0, 2, 1, 3)).reshape(row_count, head_width).astype(jnp.bfloat16)
    )
    partial_value = jnp.dot(attended, w_out, preferred_element_type=jnp.float32)
    mixed_rows = lax.psum_scatter(
        partial_value.astype(jnp.bfloat16), "tp", scatter_dimension=0, tiled=True
    )
    slot_index = positions[None, :] - filled[:, None]
    inside = (slot_index >= 0) & (slot_index < PROPS)
    selector = (slot_index[:, :, None] == jnp.arange(PROPS, dtype=jnp.int32)[None, None, :]).astype(
        jnp.bfloat16
    )
    placed_keys = jnp.einsum(
        "bpj,bjc->bpc",
        selector,
        new_keys.reshape(seq_count, PROPS, head_width),
        preferred_element_type=jnp.float32,
    ).astype(jnp.bfloat16)
    placed_values = jnp.einsum(
        "bpj,bjc->bpc",
        selector,
        new_values.reshape(seq_count, PROPS, head_width),
        preferred_element_type=jnp.float32,
    ).astype(jnp.bfloat16)
    keys_out = jnp.where(inside[:, :, None], placed_keys, keys_cache)
    values_out = jnp.where(inside[:, :, None], placed_values, values_cache)
    return (mixed_rows, keys_out, values_out)


def solution(mesh):
    placed = (
        P(None, "kv"),
        P("kv"),
        P("kv", "tp"),
        P("kv", "tp"),
        P("kv", "tp"),
        P(),
        P(),
        P("tp", "kv"),
        P(None, "kv", "tp"),
        P(None, "kv", "tp"),
        P(None, "tp", "kv"),
        P(),
        P(),
        P(),
    )
    return jax.shard_map(
        shards,
        mesh=mesh,
        in_specs=placed,
        out_specs=(P("tp", "kv"), P(None, "kv", "tp"), P(None, "kv", "tp")),
        check_vma=False,
    )
```

profile of v0, /device:TPU:0, one launch (start us, length us, event | category | flops | bytes accessed | tf_op | source)
XLA Modules:
  0.0 252.3 jit_solution(12036596136447176376)
XLA Ops:
  7.2 0.0 all-reduce.7.cloned.1.call-start
  7.2 0.8 copy-done
  8.1 1.8 convolution_convert_fusion.1
  9.9 1.9 convolution_convert_fusion.2
  11.8 1.9 convolution_convert_fusion.3
  13.7 0.0 all-reduce.7.cloned.1.call-update
  13.7 0.0 all-reduce.5.cloned.1.call-start
  13.8 1.1 fusion.13
  14.9 0.7 compare_and_fusion.2
  15.6 0.1 copy.89
  15.7 0.1 reshape.291
  15.9 2.4 gather_fusion
  18.2 0.1 gather.7
  18.3 0.1 fusion.36
  18.5 0.9 convolution_convert_fusion.4
  19.3 23.2 %all-reduce = (bf16[384]{0:T(512)(128)(2,1)S(1)}, bf16[384,4]{0,1:T(4,128)(2,1)S(1)}) all-reduce(bf16[384]{0:T(512)(128)(2,1)S(1)} %fusion.13, bf16[384,4]{0,1:T(4,128)(2,1)S(1)} %convolution_convert_fusion.4), channel_id=1, replica_groups=mesh['kv'=8,'tp'=4] {'kv'}, use_global_device_ids=true, to_apply=%region_1.0 | all-reduce | flops 1920 | bytes 7680 | tf_op jit(solution)/shard_map/psum | solution.py:66
  42.6 0.1 dynamic_slice.8
  42.7 0.1 fusion.38
  42.8 0.1 reshape.284
  42.9 0.1 copy.84
  43.0 0.4 convolution_minimum_fusion.4
  43.4 0.3 convolution_minimum_fusion.3
  43.7 0.3 convolution_minimum_fusion.2
  44.0 0.3 convolution_minimum_fusion.1
  44.3 0.3 compare_and_fusion
  44.7 0.4 convolution_add_fusion.1
  45.1 0.1 copy.91
  45.2 0.2 copy.85
  45.4 8.7 %copy.82 = bf16[24,512,256]{1,2,0:T(8,128)(2,1)} copy(bf16[24,512,256]{2,1,0:T(8,128)(2,1)} %param.22) | data formatting | bytes 12582912 | tf_op args[8]
  54.0 8.6 %copy.93 = bf16[24,512,256]{1,2,0:T(8,128)(2,1)} copy(bf16[24,512,256]{2,1,0:T(8,128)(2,1)} %param.23) | data formatting | bytes 12582912 | tf_op args[9]
  62.7 0.7 compare_and_fusion.1
  63.4 0.7 broadcast_subtract_fusion
  64.1 26.3 %all-reduce.7.cloned.1.call-done = (bf16[384,256]{1,0:T(8,128)(2,1)}, bf16[384,256]{1,0:T(8,128)(2,1)}, bf16[384,256]{1,0:T(8,128)(2,1)}) async-done(((bf16[384,256]{1,0:T(8,128)(2,1)}, bf16[384,256]{1,0:T(8,128)(2,1)}, bf16[384,256]{1,0:T(8,128)(2,1)}), (bf16[384,256]{1,0:T(8,128)(2,1)}, bf16[384,256]{1,0:T(8,128)(2,1)}, bf16[384,256]{1,0:T(8,128)(2,1)})) %all-reduce.7.cloned.1.call-update) | async-done | bytes 589840 | tf_op jit(solution)/shard_map/psum | solution.py:56
  90.4 1.9 multiply_convert_fusion.1
  92.3 0.2 reshape.281
  92.6 0.5 copy-done.6
  93.0 0.2 reshape.283
  93.2 0.1 copy-done.4
  93.3 0.3 fusion.17
  93.7 0.6 copy.88
  94.2 0.2 fusion.12
  94.4 0.7 copy.92
  95.1 4.1 %fusion = (f32[24,4,16]{2,1,0:T(4,128)S(1)}, f32[24,4,16,512]{3,2,1,0:T(8,128)S(1)}) fusion(f32[24,4,512]{2,1,0:T(4,128)S(1)} %copy-done.1, pred[24,512]{1,0:T(8,128)(4,1)S(1)} %get-tuple-element.17, bf16[24,512,4,64]{1,3,2,0:T(8,128)(2,1)} %bitcast.31, bf16[24,16,4,64]{3,2,1,0:T(4,128)(2,1)} %copy-done.4), kind=kOutput, calls=%fused_computation.5 | convolution fusion | flops 103807488 | bytes 9848832 | tf_op jit(solution)/shard_map/bihd,bphd->bhip/dot_general | solution.py:95
  99.3 0.7 copy.94
  100.0 36.4 %pmax.7 = f32[24,4,16]{2,1,0:T(4,128)} all-reduce(f32[24,4,16]{2,1,0:T(4,128)S(1)} %max.25), channel_id=1, replica_groups=mesh['kv'=8,'tp'=4] {'kv'}, use_global_device_ids=true, to_apply=%region_7.8 | all-reduce | flops 1536 | bytes 12288 | tf_op jit(solution)/shard_map/pmax | solution.py:125
  136.4 2.6 %fusion.1 = f32[24,4,16]{2,1,0:T(4,128)} fusion(f32[24,4,16,512]{3,2,1,0:T(8,128)S(1)} %get-tuple-element.22, f32[24,4,16]{2,1,0:T(4,128)S(1)} %max.25, f32[24,4,512]{2,1,0:T(4,128)S(1)} %copy-done.1, pred[24,512]{1,0:T(8,128)(4,1)} %copy-done.16), kind=kLoop, calls=%fused_computation.6 | loop fusion | flops 4717056 | bytes 3366912 | tf_op jit(solution)/shard_map/reduce_sum | solution.py:111
  139.0 1.5 fusion.24
  140.5 1.5 copy.97
  142.0 2.4 copy.95
  144.3 5.5 %fusion.3 = f32[24,4,16,64]{3,2,1,0:T(8,128)} fusion(bf16[24,512,4,64]{1,3,2,0:T(8,128)(2,1)} %bitcast.32, f32[24,4,16,512]{3,2,1,0:T(8,128)S(1)} %get-tuple-element.22, f32[24,4,16]{2,1,0:T(4,128)S(1)} %max.25, f32[24,4,512]{2,1,0:T(4,128)S(1)} %copy-done.1, pred[24,512]{1,0:T(8,128)(4,1)} %copy-done.16), kind=kOutput, calls=%fused_computation.8 | convolution fusion | flops 105381888 | bytes 10045440 | tf_op jit(solution)/shard_map/bhip,bphd->bhid/dot_general | solution.py:112
  149.8 1.2 reshape.286
  151.0 1.6 fusion.11
  152.6 0.9 multiply_convert_fusion.4
  153.5 1.0 multiply_convert_fusion
  154.6 0.0 reduce-scatter.2.cloned.1.call-start
  154.7 8.3 %convert_select_fusion = bf16[24,512,256]{2,1,0:T(8,128)(2,1)} fusion(bf16[24,512,256]{2,1,0:T(8,128)(2,1)} %param.23, pred[24,512]{1,0:T(8,128)(4,1)S(1)} %copy-done.15, bf16[24,16,256]{2,1,0:T(8,128)(2,1)S(1)} %bitcast.34, s32[24,512]{1,0:T(8,128)S(1)} %copy-done.9), kind=kOutput, calls=%fused_computation.1 | convolution fusion | flops 107151360 | bytes 12840960 | tf_op jit(solution)/shard_map/bpj,bjc->bpc/dot_general | solution.py:152
  162.9 33.2 %psum.55 = bf16[24,4,16]{2,1,0:T(4,128)(2,1)S(1)} all-reduce(bf16[24,4,16]{2,1,0:T(4,128)(2,1)S(1)} %get-tuple-element.8), channel_id=1, replica_groups=mesh['kv'=8,'tp'=4] {'kv'}, use_global_device_ids=true, to_apply=%region_12.13 | all-reduce | flops 1536 | bytes 6144 | tf_op jit(solution)/shard_map/psum | solution.py:128
  196.1 27.8 %all-reduce.5.cloned.1.call-done = bf16[24,4,16,64]{3,2,1,0:T(8,128)(2,1)} async-done(((bf16[24,4,16,64]{3,2,1,0:T(8,128)(2,1)}), bf16[24,4,16,64]{3,2,1,0:T(8,128)(2,1)}) %all-reduce.5.cloned.1.call-update) | async-done | bytes 196624 | tf_op jit(solution)/shard_map/psum | solution.py:129
  223.9 1.3 fusion.15
  225.2 0.2 copy.98
  225.4 0.3 convert_element_type.125
  225.7 0.9 convolution_convert_fusion
  226.6 8.2 %convert_select_fusion.1 = bf16[24,512,256]{2,1,0:T(8,128)(2,1)} fusion(bf16[24,512,256]{2,1,0:T(8,128)(2,1)} %param.22, pred[24,512]{1,0:T(8,128)(4,1)S(1)} %copy-done.15, bf16[24,16,256]{2,1,0:T(8,128)(2,1)S(1)} %bitcast.33, s32[24,512]{1,0:T(8,128)S(1)} %copy-done.9), kind=kOutput, calls=%fused_computation.2 | convolution fusion | flops 107151360 | bytes 12840960 | tf_op jit(solution)/shard_map/bpj,bjc->bpc/dot_general | solution.py:146
  234.8 11.0 %reduce-scatter.2.cloned.1.call-done = bf16[96,256]{1,0:T(8,128)(2,1)} async-done(((bf16[384,256]{1,0:T(8,128)(2,1)}), bf16[96,256]{1,0:T(8,128)(2,1)}) %reduce-scatter.2.cloned.1.call-update) | async-done | bytes 49168 | tf_op jit(solution)/shard_map/reduce_scatter | solution.py:138
  (51 shorter events, 0.2 us)
Async XLA Ops:
  7.2 0.9 copy-start
  7.2 8.6 %copy-start.1 = (f32[24,4,512]{2,1,0:T(4,128)S(1)}, f32[24,4,512]{2,1,0:T(4,128)}, u32[]{:S(2)}) copy-start(f32[24,4,512]{2,1,0:T(4,128)} %param.24) | copy-start | bytes 589828
  7.2 83.2 %all-reduce.7.cloned.1.call-start = ((), (), s32[]{:S(2)}) async-start(), calls=%async_computation.3 | async-start | bytes 1179648 | tf_op jit(solution)/shard_map/psum | solution.py:56
  13.7 210.2 %all-reduce.5.cloned.1.call-start = ((), (), s32[]{:S(2)}) async-start(), calls=%async_computation.1 | async-start | bytes 786432 | tf_op jit(solution)/shard_map/psum | solution.py:129
  15.8 2.6 %copy-start.5 = (bf16[384,256]{1,0:T(8,128)(2,1)S(1)}, bf16[384,256]{1,0:T(8,128)(2,1)}, u32[]{:S(2)}) copy-start(bf16[384,256]{1,0:T(8,128)(2,1)} %param.14) | copy-start | bytes 589828
  15.8 2.6 %copy-start.17 = (f32[256]{0:T(256)S(1)}, f32[256]{0:T(256)}, u32[]{:S(2)}) copy-start(f32[256]{0:T(256)} %param.15) | copy-start | bytes 3076
  15.9 26.7 %copy-start.19 = (f32[16]{0:T(128)S(1)}, f32[16]{0:T(128)}, u32[]{:S(2)}) copy-start(f32[16]{0:T(128)} %param.20) | copy-start | bytes 196
  15.9 27.0 %copy-start.18 = (s32[24,16]{0,1:T(8,128)S(1)}, s32[24,16]{0,1:T(8,128)}, u32[]{:S(2)}) copy-start(s32[24,16]{0,1:T(8,128)} %param.27) | copy-start | bytes 4612
  45.4 48.8 %copy-start.10 = (pred[24,16,16]{0,2,1:T(8,128)(4,1)}, pred[24,16,16]{0,2,1:T(8,128)(4,1)S(1)}, u32[]{:S(2)}) copy-start(pred[24,16,16]{0,2,1:T(8,128)(4,1)S(1)} %copy.85) | copy-start | bytes 18436
  63.4 35.8 %copy-start.16 = (pred[24,512]{1,0:T(8,128)(4,1)}, pred[24,512]{1,0:T(8,128)(4,1)S(1)}, u32[]{:S(2)}) copy-start(pred[24,512]{1,0:T(8,128)(4,1)S(1)} %get-tuple-element.17) | copy-start | bytes 36868
  92.3 0.7 copy-start.6
  92.6 0.8 copy-start.4
  94.2 0.9 copy-start.2
  95.1 4.1 %copy-start.12 = (f32[24,4,16]{2,1,0:T(4,128)S(1)}, f32[24,4,16]{2,1,0:T(4,128)}, u32[]{:S(2)}) copy-start(f32[24,4,16]{2,1,0:T(4,128)} %copy.92) | copy-start | bytes 18436
  136.4 2.6 %copy-start.3 = (f32[24,4,16,16]{0,3,2,1:T(8,128)S(1)}, f32[24,4,16,16]{0,3,2,1:T(8,128)}, u32[]{:S(2)}) copy-start(f32[24,4,16,16]{0,3,2,1:T(8,128)} %copy-done.2) | copy-start | bytes 294916
  136.4 2.6 %copy-start.11 = (pred[24,16,16]{0,2,1:T(8,128)(4,1)S(1)}, pred[24,16,16]{0,2,1:T(8,128)(4,1)}, u32[]{:S(2)}) copy-start(pred[24,16,16]{0,2,1:T(8,128)(4,1)} %copy-done.10) | copy-start | bytes 18436
  136.4 2.6 %copy-start.13 = (f32[24,4,16]{0,2,1:T(8,128)S(1)}, f32[24,4,16]{0,2,1:T(8,128)}, u32[]{:S(2)}) copy-start(f32[24,4,16]{0,2,1:T(8,128)} %copy.94) | copy-start | bytes 18436
  149.8 4.8 %copy-start.8 = (bf16[384,256]{1,0:T(8,128)(2,1)S(1)}, bf16[384,256]{1,0:T(8,128)(2,1)}, u32[]{:S(2)}) copy-start(bf16[384,256]{1,0:T(8,128)(2,1)} %get-tuple-element.18) | copy-start | bytes 589828
  149.8 4.8 %copy-start.9 = (s32[24,512]{1,0:T(8,128)S(1)}, s32[24,512]{1,0:T(8,128)}, u32[]{:S(2)}) copy-start(s32[24,512]{1,0:T(8,128)} %broadcast_subtract_fusion) | copy-start | bytes 147460
  149.8 4.8 %copy-start.15 = (pred[24,512]{1,0:T(8,128)(4,1)S(1)}, pred[24,512]{1,0:T(8,128)(4,1)}, u32[]{:S(2)}) copy-start(pred[24,512]{1,0:T(8,128)(4,1)} %get-tuple-element.16) | copy-start | bytes 36868
  154.6 91.2 %reduce-scatter.2.cloned.1.call-start = ((), (), s32[]{:S(2)}) async-start(), calls=%async_computation.2 | async-start | bytes 245760 | tf_op jit(solution)/shard_map/reduce_scatter | solution.py:138
  154.7 71.0 %copy-start.14 = (bf16[256,256]{1,0:T(8,128)(2,1)S(1)}, bf16[256,256]{1,0:T(8,128)(2,1)}, u32[]{:S(2)}) copy-start(bf16[256,256]{1,0:T(8,128)(2,1)} %param.21) | copy-start | bytes 393220
  162.9 63.6 %copy-start.7 = (bf16[384,256]{1,0:T(8,128)(2,1)S(1)}, bf16[384,256]{1,0:T(8,128)(2,1)}, u32[]{:S(2)}) copy-start(bf16[384,256]{1,0:T(8,128)(2,1)} %copy-done.6) | copy-start | bytes 589828
Sparse Core Ops, SparseCore 0:
  13.8 76.5 all-reduce.6
  154.7 69.1 all-reduce.4
  226.9 18.7 reduce-scatter.1
where the time goes:
time: 254 us; the launch traced here: 252 us
  blocking collectives  92.9 us (37%)
  waiting for transfers between devices  65.1 us (26%)
  matrix products  37.5 us (15%)
  local copies, waits for them, and re-layouts  29.7 us (12%)
  between operations  14.2 us (6%)
  other arithmetic  12.7 us (5%)
    pmax x1, blocking collectives, shards(): top_score = lax.pmax(local_max, 'kv')  36.4 us
    psum x1, blocking collectives, shards(): lax.psum((rescale * local_sum).astype(jnp.bfloat16), 'kv')  33.2 us
    psum x1, waiting for transfers between devices, shards(): lax.psum((rescale[..., None] * local_values).astype(jnp.bfloat16), 'kv')  27.8 us
    psum x1, waiting for transfers between devices, shards(): lax.psum(jnp.dot(scaled, w_query, preferred_element_type=jnp.float32).ast...  26.3 us
    psum x1, blocking collectives, shards(): lax.psum(square_part.astype(jnp.bfloat16), 'kv').astype(jnp.float32)  23.2 us
    unnamed x45, local copies, waits for them, and re-layouts  18.8 us
    reduce_scatter x1, waiting for transfers between devices, shards(): lax.psum_scatter(partial_value.astype(jnp.bfloat16), 'tp', scatter_dimens...  11 us
    dot_general x1, matrix products, shards(): jnp.einsum('bpj,bjc->bpc', selector, new_values.reshape(seq_count, PROPS,...  8.26 us
  transfers between devices with their start and end apart: 3, of which 3 were waited for; matrix products, arithmetic and copies ran while one was open for 17% of the time, Pallas kernels for 0%

commit v1 on v0

--- a/solution.py
+++ b/solution.py
@@ -53,8 +53,12 @@
     gate_part = jnp.dot(scaled, gate_cols, preferred_element_type=jnp.float32)
     bias_local = lax.dynamic_slice_in_dim(gate_bias, tp_index * head_count, head_count, 0)
     query_sum, key_sum, value_sum, gate_sum, square_sum = (
-        lax.psum(
-            jnp.dot(scaled, w_query, preferred_element_type=jnp.float32).astype(jnp.bfloat16), "kv"
+        jnp.sum(
+            lax.all_gather(
+                jnp.dot(scaled, w_query, preferred_element_type=jnp.float32).astype(jnp.bfloat16),
+                "kv",
+            ),
+            axis=0,
         ).astype(jnp.float32),
         lax.psum(
             jnp.dot(scaled, w_key, preferred_element_type=jnp.float32).astype(jnp.bfloat16), "kv"

time: 254 us -> 290 us (1.14)
  waiting for transfers between devices: 65.1 us -> 104 us
    all_gather x0 -> x1, waiting for transfers between devices: none -> 43.1 us  [shards(): lax.all_gather(jnp.dot(scaled, w_query, preferred_element_type=jnp.float3...]
    psum x1, waiting for transfers between devices: 26.3 us -> 22.7 us  [shards(): lax.psum(jnp.dot(scaled, w_key, preferred_element_type=jnp.float32).astyp...]
    unnamed x45 -> x57, local copies, waits for them, and re-layouts: 18.8 us -> 19.1 us
  transfers between devices with their start and end apart: 3 -> 4, of which waited for: 3 -> 4; matrix products, arithmetic and copies ran while one was open for 17% -> 16% of each run, Pallas kernels for 0% -> 0%
where the time goes in v1:
time: 290 us; the launch traced here: 289 us
  waiting for transfers between devices  104 us (36%)
  blocking collectives  92.3 us (32%)
  matrix products  34.8 us (12%)
  local copies, waits for them, and re-layouts  29.9 us (10%)
  between operations  14.3 us (5%)
  other arithmetic  13.2 us (5%)
    all_gather x1, waiting for transfers between devices, shards(): lax.all_gather(jnp.dot(scaled, w_query, preferred_element_type=jnp.float3...  43.1 us
    pmax x1, blocking collectives, shards(): top_score = lax.pmax(local_max, 'kv')  35.5 us
    psum x1, blocking collectives, shards(): lax.psum((rescale * local_sum).astype(jnp.bfloat16), 'kv')  33.6 us
    psum x1, waiting for transfers between devices, shards(): lax.psum((rescale[..., None] * local_values).astype(jnp.bfloat16), 'kv')  27.3 us
    psum x1, blocking collectives, shards(): lax.psum(square_part.astype(jnp.bfloat16), 'kv').astype(jnp.float32)  23.1 us
    psum x1, waiting for transfers between devices, shards(): lax.psum(jnp.dot(scaled, w_key, preferred_element_type=jnp.float32).astyp...  22.7 us
    unnamed x57, local copies, waits for them, and re-layouts  19.1 us
    reduce_scatter x1, waiting for transfers between devices, shards(): lax.psum_scatter(partial_value.astype(jnp.bfloat16), 'tp', scatter_dimens...  10.8 us
  transfers between devices with their start and end apart: 4, of which 4 were waited for; matrix products, arithmetic and copies ran while one was open for 16% of the time, Pallas kernels for 0%

profile of v1, /device:TPU:0, one launch (start us, length us, event | category | flops | bytes accessed | tf_op | source)
XLA Modules:
  0.0 288.6 jit_solution(4079631779908832907)
XLA Ops:
  7.2 0.8 copy-done
  8.1 1.8 convolution_convert_fusion.1
  9.9 1.9 convolution_convert_fusion.2
  11.8 0.0 all-gather.3.cloned.1.call-start
  11.9 1.9 convolution_convert_fusion.3
  13.8 0.0 all-reduce.5.cloned.1.call-start
  13.9 1.1 fusion.13
  14.9 0.7 compare_and_fusion.2
  15.7 0.1 copy.87
  15.8 0.1 reshape.297
  15.9 2.4 gather_fusion
  18.3 0.1 gather.7
  18.4 0.9 convolution_convert_fusion.4
  19.3 23.1 %all-reduce = (bf16[384]{0:T(512)(128)(2,1)S(1)}, bf16[384,4]{0,1:T(4,128)(2,1)S(1)}) all-reduce(bf16[384]{0:T(512)(128)(2,1)S(1)} %fusion.13, bf16[384,4]{0,1:T(4,128)(2,1)S(1)} %convolution_convert_fusion.4), channel_id=1, replica_groups=mesh['kv'=8,'tp'=4] {'kv'}, use_global_device_ids=true, to_apply=%region_1.0 | all-reduce | flops 1920 | bytes 7680 | tf_op jit(solution)/shard_map/psum | solution.py:70
  42.5 0.1 dynamic_slice.8
  42.5 0.1 mul.79
  42.6 0.1 fusion.38
  42.7 0.1 reshape.289
  42.8 0.1 copy.82
  42.9 0.1 fusion.36
  43.0 0.4 convolution_minimum_fusion.4
  43.4 0.3 convolution_minimum_fusion.3
  43.7 0.3 convolution_minimum_fusion.2
  44.1 0.3 convolution_minimum_fusion.1
  44.4 0.3 compare_and_fusion
  44.7 0.4 convolution_add_fusion.1
  45.2 0.1 copy.89
  45.2 0.2 copy.83
  45.4 8.6 %copy.80 = bf16[24,512,256]{1,2,0:T(8,128)(2,1)} copy(bf16[24,512,256]{2,1,0:T(8,128)(2,1)} %param.22) | data formatting | bytes 12582912 | tf_op args[8]
  54.1 8.6 %copy.91 = bf16[24,512,256]{1,2,0:T(8,128)(2,1)} copy(bf16[24,512,256]{2,1,0:T(8,128)(2,1)} %param.23) | data formatting | bytes 12582912 | tf_op args[9]
  62.7 0.7 compare_and_fusion.1
  63.4 0.7 broadcast_subtract_fusion
  64.1 22.7 %all-reduce.7.cloned.1.call-done = (bf16[384,256]{1,0:T(8,128)(2,1)}, bf16[384,256]{1,0:T(8,128)(2,1)}) async-done(((bf16[384,256]{1,0:T(8,128)(2,1)}, bf16[384,256]{1,0:T(8,128)(2,1)}), (bf16[384,256]{1,0:T(8,128)(2,1)}, bf16[384,256]{1,0:T(8,128)(2,1)})) %all-reduce.7.cloned.1.call-update) | async-done | bytes 393232 | tf_op jit(solution)/shard_map/psum | solution.py:63
  86.8 1.2 multiply_convert_fusion.2
  87.9 0.2 reshape.288
  88.1 1.0 reshape.291
  89.1 43.1 %all-gather.3.cloned.1.call-done = bf16[3072,256]{1,0:T(8,128)(2,1)} async-done(((bf16[384,256]{1,0:T(8,128)(2,1)}), bf16[3072,256]{1,0:T(8,128)(2,1)}) %all-gather.3.cloned.1.call-update) | async-done | bytes 1572880 | tf_op jit(solution)/shard_map/all_gather | solution.py:57
  132.2 1.7 reduce_sum.40
  133.9 0.3 reshape.294
  134.2 0.5 multiply_convert_fusion.1
  134.7 0.7 copy-done.4
  135.5 0.3 fusion.17
  135.8 0.6 copy.86
  136.4 0.2 fusion.12
  136.6 0.7 copy.90
  137.3 4.1 %fusion = (f32[24,4,16]{2,1,0:T(4,128)S(1)}, f32[24,4,16,512]{3,2,1,0:T(8,128)S(1)}) fusion(f32[24,4,512]{2,1,0:T(4,128)S(1)} %copy-done.1, pred[24,512]{1,0:T(8,128)(4,1)S(1)} %get-tuple-element.16, bf16[24,512,4,64]{1,3,2,0:T(8,128)(2,1)} %bitcast.32, bf16[24,16,4,64]{3,2,1,0:T(4,128)(2,1)} %copy-done.4), kind=kOutput, calls=%fused_computation.5 | convolution fusion | flops 103807488 | bytes 9848832 | tf_op jit(solution)/shard_map/bihd,bphd->bhip/dot_general | solution.py:99
  141.4 0.7 copy.92
  142.1 35.5 %pmax.7 = f32[24,4,16]{2,1,0:T(4,128)} all-reduce(f32[24,4,16]{2,1,0:T(4,128)S(1)} %max.25), channel_id=1, replica_groups=mesh['kv'=8,'tp'=4] {'kv'}, use_global_device_ids=true, to_apply=%region_7.8 | all-reduce | flops 1536 | bytes 12288 | tf_op jit(solution)/shard_map/pmax | solution.py:129
  177.7 2.6 fusion.1
  180.2 1.5 fusion.24
  181.7 1.4 copy.95
  183.2 2.4 copy.93
  185.6 4.0 %fusion.3 = f32[24,4,16,64]{3,2,1,0:T(8,128)S(1)} fusion(bf16[24,512,4,64]{1,3,2,0:T(8,128)(2,1)} %bitcast.33, f32[24,4,16,512]{3,2,1,0:T(8,128)S(1)} %get-tuple-element.20, f32[24,4,16]{2,1,0:T(4,128)S(1)} %max.25, f32[24,4,512]{2,1,0:T(4,128)S(1)} %copy-done.1, pred[24,512]{1,0:T(8,128)(4,1)} %copy-done.22), kind=kOutput, calls=%fused_computation.8 | convolution fusion | flops 105381888 | bytes 10045440 | tf_op jit(solution)/shard_map/bhip,bphd->bhid/dot_general | solution.py:116
  189.6 0.3 fusion.11
  190.0 1.0 multiply_convert_fusion
  191.2 8.3 %convert_select_fusion = bf16[24,512,256]{2,1,0:T(8,128)(2,1)} fusion(bf16[24,512,256]{2,1,0:T(8,128)(2,1)} %param.23, pred[24,512]{1,0:T(8,128)(4,1)S(1)} %copy-done.21, bf16[24,16,256]{2,1,0:T(8,128)(2,1)S(1)} %bitcast.35, s32[24,512]{1,0:T(8,128)S(1)} %copy-done.12), kind=kOutput, calls=%fused_computation.1 | convolution fusion | flops 107151360 | bytes 12840960 | tf_op jit(solution)/shard_map/bpj,bjc->bpc/dot_general | solution.py:156
  199.4 33.6 %psum.47 = bf16[24,4,16]{2,1,0:T(4,128)(2,1)S(1)} all-reduce(bf16[24,4,16]{2,1,0:T(4,128)(2,1)S(1)} %get-tuple-element.7), channel_id=1, replica_groups=mesh['kv'=8,'tp'=4] {'kv'}, use_global_device_ids=true, to_apply=%region_12.13 | all-reduce | flops 1536 | bytes 6144 | tf_op jit(solution)/shard_map/psum | solution.py:132
  233.0 27.3 %all-reduce.5.cloned.1.call-done = bf16[24,4,16,64]{3,2,1,0:T(8,128)(2,1)} async-done(((bf16[24,4,16,64]{3,2,1,0:T(8,128)(2,1)}), bf16[24,4,16,64]{3,2,1,0:T(8,128)(2,1)}) %all-reduce.5.cloned.1.call-update) | async-done | bytes 196624 | tf_op jit(solution)/shard_map/psum | solution.py:133
  260.3 1.3 fusion.15
  261.6 0.2 copy.96
  261.8 0.3 convert_element_type.133
  262.1 0.9 convolution_convert_fusion
  263.0 8.2 %convert_select_fusion.1 = bf16[24,512,256]{2,1,0:T(8,128)(2,1)} fusion(bf16[24,512,256]{2,1,0:T(8,128)(2,1)} %param.22, pred[24,512]{1,0:T(8,128)(4,1)S(1)} %copy-done.21, bf16[24,16,256]{2,1,0:T(8,128)(2,1)S(1)} %bitcast.34, s32[24,512]{1,0:T(8,128)S(1)} %copy-done.12), kind=kOutput, calls=%fused_computation.2 | convolution fusion | flops 107151360 | bytes 12840960 | tf_op jit(solution)/shard_map/bpj,bjc->bpc/dot_general | solution.py:150
  271.2 10.8 %reduce-scatter.2.cloned.1.call-done = bf16[96,256]{1,0:T(8,128)(2,1)} async-done(((bf16[384,256]{1,0:T(8,128)(2,1)}), bf16[96,256]{1,0:T(8,128)(2,1)}) %reduce-scatter.2.cloned.1.call-update) | async-done | bytes 49168 | tf_op jit(solution)/shard_map/reduce_scatter | solution.py:142
  (69 shorter events, 0.4 us)
Async XLA Ops:
  7.2 0.9 copy-start
  7.2 8.7 %copy-start.1 = (f32[24,4,512]{2,1,0:T(4,128)S(1)}, f32[24,4,512]{2,1,0:T(4,128)}, u32[]{:S(2)}) copy-start(f32[24,4,512]{2,1,0:T(4,128)} %param.24) | copy-start | bytes 589828
  7.2 79.6 %all-reduce.7.cloned.1.call-start = ((), (), s32[]{:S(2)}) async-start(), calls=%async_computation.4 | async-start | bytes 786432 | tf_op jit(solution)/shard_map/psum | solution.py:63
  11.8 120.4 %all-gather.3.cloned.1.call-start = ((), (), s32[]{:S(2)}) async-start(), calls=%async_computation.3 | async-start | bytes 1769472 | tf_op jit(solution)/shard_map/all_gather | solution.py:57
  13.8 246.5 %all-reduce.5.cloned.1.call-start = ((), (), s32[]{:S(2)}) async-start(), calls=%async_computation.1 | async-start | bytes 786432 | tf_op jit(solution)/shard_map/psum | solution.py:133
  15.9 2.5 copy-start.5
  15.9 2.5 copy-start.23
  15.9 26.6 %copy-start.25 = (f32[16]{0:T(128)S(1)}, f32[16]{0:T(128)}, u32[]{:S(2)}) copy-start(f32[16]{0:T(128)} %param.20) | copy-start | bytes 196
  15.9 26.9 %copy-start.24 = (s32[24,16]{0,1:T(8,128)S(1)}, s32[24,16]{0,1:T(8,128)}, u32[]{:S(2)}) copy-start(s32[24,16]{0,1:T(8,128)} %param.27) | copy-start | bytes 4612
  45.4 91.0 %copy-start.13 = (pred[24,16,16]{0,2,1:T(8,128)(4,1)}, pred[24,16,16]{0,2,1:T(8,128)(4,1)S(1)}, u32[]{:S(2)}) copy-start(pred[24,16,16]{0,2,1:T(8,128)(4,1)S(1)} %copy.83) | copy-start | bytes 18436
  63.4 73.9 %copy-start.22 = (pred[24,512]{1,0:T(8,128)(4,1)}, pred[24,512]{1,0:T(8,128)(4,1)S(1)}, u32[]{:S(2)}) copy-start(pred[24,512]{1,0:T(8,128)(4,1)S(1)} %get-tuple-element.16) | copy-start | bytes 36868
  87.9 44.3 %copy-start.6 = (bf16[384,256]{1,0:T(8,128)(2,1)}, bf16[384,256]{1,0:T(8,128)(2,1)S(1)}, u32[]{:S(2)}) copy-start(bf16[384,256]{1,0:T(8,128)(2,1)S(1)} %get-tuple-element.18) | copy-start | bytes 589828
  87.9 44.3 %copy-start.8 = (bf16[384,256]{1,0:T(8,128)(2,1)}, bf16[384,256]{1,0:T(8,128)(2,1)S(1)}, u32[]{:S(2)}) copy-start(bf16[384,256]{1,0:T(8,128)(2,1)S(1)} %get-tuple-element.17) | copy-start | bytes 589828
  134.7 0.7 copy-start.4
  136.4 0.9 copy-start.2
  137.3 4.1 %copy-start.15 = (f32[24,4,16]{2,1,0:T(4,128)S(1)}, f32[24,4,16]{2,1,0:T(4,128)}, u32[]{:S(2)}) copy-start(f32[24,4,16]{2,1,0:T(4,128)} %copy.90) | copy-start | bytes 18436
  177.7 2.6 copy-start.3
  177.7 2.6 copy-start.14
  177.7 2.6 copy-start.19
  185.6 4.0 %copy-start.10 = (bf16[24,16,4,64]{3,2,1,0:T(4,128)(2,1)S(1)}, bf16[24,16,4,64]{3,2,1,0:T(4,128)(2,1)}, u32[]{:S(2)}) copy-start(bf16[24,16,4,64]{3,2,1,0:T(4,128)(2,1)} %reshape.291) | copy-start | bytes 589828
  185.6 4.0 %copy-start.11 = (bf16[24,4,16,16]{3,2,1,0:T(8,128)(2,1)S(1)}, bf16[24,4,16,16]{3,2,1,0:T(8,128)(2,1)}, u32[]{:S(2)}) copy-start(bf16[24,4,16,16]{3,2,1,0:T(8,128)(2,1)} %copy.93) | copy-start | bytes 147460
  185.6 4.4 %copy-start.16 = (f32[24,4,16]{2,1,0:T(4,128)S(1)}, f32[24,4,16]{2,1,0:T(4,128)}, u32[]{:S(2)}) copy-start(f32[24,4,16]{2,1,0:T(4,128)} %pmax.7) | copy-start | bytes 18436
  185.6 4.4 %copy-start.17 = (f32[24,4,16]{2,1,0:T(4,128)S(1)}, f32[24,4,16]{2,1,0:T(4,128)}, u32[]{:S(2)}) copy-start(f32[24,4,16]{2,1,0:T(4,128)} %copy.95) | copy-start | bytes 18436
  185.6 4.4 %copy-start.18 = (f32[24,4,16]{2,1,0:T(4,128)S(1)}, f32[24,4,16]{2,1,0:T(4,128)}, u32[]{:S(2)}) copy-start(f32[24,4,16]{2,1,0:T(4,128)} %fusion.1) | copy-start | bytes 18436
  189.6 1.5 copy-start.9
  189.6 1.5 copy-start.12
  189.6 1.5 copy-start.21
  191.1 91.0 %reduce-scatter.2.cloned.1.call-start = ((), (), s32[]{:S(2)}) async-start(), calls=%async_computation.2 | async-start | bytes 245760 | tf_op jit(solution)/shard_map/reduce_scatter | solution.py:142
  191.2 70.9 %copy-start.20 = (bf16[256,256]{1,0:T(8,128)(2,1)S(1)}, bf16[256,256]{1,0:T(8,128)(2,1)}, u32[]{:S(2)}) copy-start(bf16[256,256]{1,0:T(8,128)(2,1)} %param.21) | copy-start | bytes 393220
  199.4 63.6 %copy-start.7 = (bf16[384,256]{1,0:T(8,128)(2,1)S(1)}, bf16[384,256]{1,0:T(8,128)(2,1)}, u32[]{:S(2)}) copy-start(bf16[384,256]{1,0:T(8,128)(2,1)} %copy-done.6) | copy-start | bytes 589828
Sparse Core Ops, SparseCore 0:
  12.0 74.7 all-reduce.6
  88.9 43.2 all-gather.2
  191.2 69.1 all-reduce.4
  263.2 18.8 reduce-scatter.1
